TPU v7x, 256 devices: a whole 4x4x8 slice. The times are simulated.
256 devices in a mesh: sp: 32 (over z, y), tp: 8 (over x, core).
Axes of the slice: x: 4, y: 4, z: 8, core: 2. Of those that a mesh axis runs over, the one named last changes fastest.
Arguments:
- activations: bfloat16 [24576, 2048], P(('sp', 'tp')), may hold values from -6 to 6
- in_gain: float32 [2048], replicated, may hold values from 0.1 to 1.9
- w_pool_in: bfloat16 [2048, 1024], P(None, 'tp'), may hold values from -0.125 to 0.125
- pool_gain: float32 [1024], P('tp'), may hold values from 0.1 to 1.9
- w_qlat: bfloat16 [2048, 768], P(None, 'tp'), may hold values from -0.125 to 0.125
- w_kvlat: bfloat16 [2048, 512], P(None, 'tp'), may hold values from -0.125 to 0.125
- w_krope: bfloat16 [2048, 32], replicated, may hold values from -0.125 to 0.125
- qlat_gain: float32 [768], replicated, may hold values from 0.1 to 1.9
- kvlat_gain: float32 [512], replicated, may hold values from 0.1 to 1.9
- w_qup: bfloat16 [768, 1536], P(None, 'tp'), may hold values from -0.21875 to 0.21875
- w_kup: bfloat16 [512, 1024], P(None, 'tp'), may hold values from -0.25 to 0.25
- w_vup: bfloat16 [512, 1024], P(None, 'tp'), may hold values from -0.25 to 0.25
- qhead_gain: float32 [96], replicated, may hold values from 1.1 to 1.9
- khead_gain: float32 [96], replicated, may hold values from 1.1 to 1.9
- w_out_pool: bfloat16 [1024, 2048], P('tp'), may hold values from -0.1875 to 0.1875
- w_out_attn: bfloat16 [1024, 2048], P('tp'), may hold values from -0.75 to 0.75
Outputs:
- mixed: bfloat16 [24576, 2048], P(('sp', 'tp'))
All inputs are finite; a program needn't handle non-finite values.
Results may differ from a plain program's by a relative error of at most 0.025.
Values may be sent and summed in bfloat16 or wider, within the bound.
No kernel may reach another device: no remote copies, remote signals or barrier semaphores. Data moves between devices by JAX's collectives and lax.ppermute only.
A program may use at most 128 MiB of HBM per device.

v0:
```python
import math
import jax
import jax.numpy as jnp
from jax import lax
from jax.sharding import PartitionSpec as P

GROUP = 256
NOPE = 64
ROPE = 32
VDIM = 64
QLAT = 768
KVLAT = 512
norm_eps = 1e-06
rope_theta = 10000.0
rim_depth = 15
block_rows = 512


def from_behind(block, axis, distance):
    devices = range(lax.axis_size(axis))
    route = [(i - distance, i) for i in devices if i - distance in devices]
    return lax.ppermute(block, axis, route)


def copy_for_each(x, axis):
    copies = jnp.broadcast_to(x, (lax.axis_size(axis), *x.shape))
    return lax.all_to_all(copies, axis, split_axis=0, concat_axis=0, tiled=True)


def of_everyone(x, axis):
    everything = copy_for_each(x, axis)
    return jnp.sum(everything, axis=0)


def together(arrays, axis):
    ends = [0]
    for a in arrays:
        ends.append(ends[-1] + a.size)
    running = of_everyone(jnp.concatenate([a.ravel() for a in arrays]), axis)
    return tuple((running[b:e].reshape(a.shape) for a, b, e in zip(arrays, ends, ends[1:])))


def side_by_side(arrays, axis, dim, along):
    widths = [a.shape[along] for a in arrays]
    both = jnp.concatenate(arrays, axis=along)
    filled = lax.all_gather(both, axis, axis=dim, tiled=True)
    return tuple(jnp.split(filled, [sum(widths[:k]) for k in range(1, len(widths))], axis=along))


def row_norm(source, norm_gain):
    as_float = source.astype(jnp.float32)
    factor = lax.rsqrt(jnp.mean(as_float * as_float, axis=-1, keepdims=True) + norm_eps)
    return as_float * factor * norm_gain


def rotate(head_rows, positions):
    half_rope = ROPE // 2
    frequency = rope_theta ** (-jnp.arange(0, ROPE, 2, dtype=jnp.float32) / ROPE)
    angles = positions.astype(jnp.float32)[:, None] * frequency[None, :]
    cosine = jnp.cos(angles)[:, None, :]
    sine_part = jnp.sin(angles)[:, None, :]
    plain_part = head_rows[..., :NOPE]
    lower_half = head_rows[..., NOPE : NOPE + half_rope]
    upper_half = head_rows[..., NOPE + half_rope :]
    return jnp.concatenate(
        [
            plain_part,
            lower_half * cosine - upper_half * sine_part,
            upper_half * cosine + lower_half * sine_part,
        ],
        axis=-1,
    )


def pool_mix(extended, positions, channel_start):
    row_count = positions.shape[0]
    width = extended.shape[1]
    channel = channel_start + jnp.arange(width, dtype=jnp.int32)
    window = jnp.left_shift(jnp.int32(2), channel // GROUP)
    as_float = extended.astype(jnp.float32)
    window_sum = jnp.zeros((row_count, width), jnp.float32)
    for lag_index in range(rim_depth + 1):
        lagged = as_float[rim_depth - lag_index : rim_depth - lag_index + row_count]
        window_sum = window_sum + jnp.where(lag_index < window[None, :], lagged, 0.0)
    divisor = jnp.minimum(positions[:, None] + 1, window[None, :]).astype(jnp.float32)
    return window_sum / divisor - as_float[rim_depth:]


def make_queries(q_normed, w_qup, norm_gain, positions):
    row_count = q_normed.shape[0]
    head_count = w_qup.shape[1] // (NOPE + ROPE)
    query_raw = jnp.dot(q_normed, w_qup, preferred_element_type=jnp.float32).astype(jnp.bfloat16)
    query_raw = query_raw.reshape(row_count, head_count, NOPE + ROPE)
    return rotate(row_norm(query_raw, norm_gain), positions).astype(jnp.bfloat16)


def plain_parts(kv_rows, w_kup, w_vup):
    key_plain = jnp.dot(kv_rows, w_kup, preferred_element_type=jnp.float32).astype(jnp.bfloat16)
    value_rows = jnp.dot(kv_rows, w_vup, preferred_element_type=jnp.float32).astype(jnp.bfloat16)
    return (key_plain, value_rows)


def finish_keys(key_plain, rope_rows, norm_gain, positions):
    row_count = key_plain.shape[0]
    head_count = key_plain.shape[1] // NOPE
    key_plain = key_plain.reshape(row_count, head_count, NOPE)
    shared = jnp.broadcast_to(rope_rows[:, None, :], (row_count, head_count, ROPE))
    joined = jnp.concatenate([key_plain, shared], axis=-1)
    key_rows = rotate(row_norm(joined, norm_gain), positions).astype(jnp.bfloat16)
    return key_rows.reshape(row_count, head_count * (NOPE + ROPE))


def update(state_pair, queries, query_pos, key_rows, value_rows, key_pos):
    numerator, denominator = state_pair
    head_count = queries.shape[1]
    key_rows = key_rows.reshape(key_rows.shape[0], head_count, NOPE + ROPE)
    value_rows = value_rows.reshape(value_rows.shape[0], head_count, VDIM)
    scores = jnp.einsum("qhd,khd->hqk", queries, key_rows, preferred_element_type=jnp.float32)
    scores = scores * (NOPE + ROPE) ** (-0.5)
    weights = jnp.where(key_pos[None, None, :] <= query_pos[None, :, None], jnp.exp(scores), 0.0)
    denominator = denominator + jnp.sum(weights, axis=-1)
    numerator = numerator + jnp.einsum(
        "hqk,khd->qhd", weights.astype(jnp.bfloat16), value_rows, preferred_element_type=jnp.float32
    )
    return (numerator, denominator)


def sweep(state_pair, pieces, expand, queries, query_pos):
    shard_rows = queries.shape[0]
    piece_rows = pieces[0].shape[0]
    block_size = shard_rows * math.gcd(piece_rows // shard_rows, max(1, block_rows // shard_rows))

    def advance(block_index, current):
        offset = block_index * block_size

        def accumulate(inner):
            chosen = tuple(
                (lax.dynamic_slice_in_dim(member, offset, block_size, 0) for member in pieces)
            )
            key_pos = offset + jnp.arange(block_size, dtype=jnp.int32)
            key_rows, value_rows = expand(chosen, key_pos)
            return update(inner, queries, query_pos, key_rows, value_rows, key_pos)

        def unchanged(inner):
            return inner

        return lax.cond(offset <= query_pos[-1], accumulate, unchanged, current)

    return lax.fori_loop(0, piece_rows // block_size, advance, state_pair)


def local(
    activations,
    in_gain,
    w_pool_in,
    pool_gain,
    w_qlat,
    w_kvlat,
    w_krope,
    qlat_gain,
    kvlat_gain,
    w_qup,
    w_kup,
    w_vup,
    qhead_gain,
    khead_gain,
    w_out_pool,
    w_out_attn,
):
    own_input = lax.all_gather(activations, "tp", axis=0, tiled=True)
    row_count = own_input.shape[0]
    positions = lax.axis_index("sp") * row_count + jnp.arange(row_count, dtype=jnp.int32)
    normed = row_norm(own_input, in_gain).astype(jnp.bfloat16)
    pool_in = jnp.dot(normed, w_pool_in, preferred_element_type=jnp.float32).astype(jnp.bfloat16)
    prev_rows = from_behind(pool_in[row_count - rim_depth :], "sp", 1)
    extended = jnp.concatenate([prev_rows, pool_in], axis=0)
    channel_start = lax.axis_index("tp") * pool_in.shape[1]
    pool_out = (pool_mix(extended, positions, channel_start) * pool_gain).astype(jnp.bfloat16)
    q_part = jnp.dot(normed, w_qlat, preferred_element_type=jnp.float32).astype(jnp.bfloat16)
    kv_part = jnp.dot(normed, w_kvlat, preferred_element_type=jnp.float32).astype(jnp.bfloat16)
    rope_key = jnp.dot(normed, w_krope, preferred_element_type=jnp.float32).astype(jnp.bfloat16)
    tp_index = lax.axis_index("tp")
    q_width = q_part.shape[1]
    kv_width = kv_part.shape[1]
    q_float = q_part.astype(jnp.float32)
    kv_float = kv_part.astype(jnp.float32)
    q_squares, kv_squares = together(
        (jnp.sum(q_float * q_float, axis=1), jnp.sum(kv_float * kv_float, axis=1)), "tp"
    )
    q_gain = lax.dynamic_slice_in_dim(qlat_gain, tp_index * q_width, q_width)
    kv_gain = lax.dynamic_slice_in_dim(kvlat_gain, tp_index * kv_width, kv_width)
    q_scaled = q_float * lax.rsqrt(q_squares / QLAT + norm_eps)[:, None] * q_gain
    kv_scaled = kv_float * lax.rsqrt(kv_squares / KVLAT + norm_eps)[:, None] * kv_gain
    q_normed, kv_normed = (
        lax.all_gather(q_scaled.astype(jnp.bfloat16), "tp", axis=1, tiled=True),
        lax.all_gather(kv_scaled.astype(jnp.bfloat16), "tp", axis=1, tiled=True),
    )
    queries = make_queries(q_normed, w_qup, qhead_gain, positions)
    head_count = queries.shape[1]
    start_pair = (
        jnp.zeros((row_count, head_count, VDIM), jnp.float32),
        jnp.zeros((head_count, row_count), jnp.float32),
    )
    key_plain, value_rows = plain_parts(kv_normed, w_kup, w_vup)

    def expand_plain(chosen, key_pos):
        return (finish_keys(chosen[0], chosen[2], khead_gain, key_pos), chosen[1])

    numerator, denominator = sweep(
        start_pair,
        side_by_side((key_plain, value_rows, rope_key), "sp", 0, 1),
        expand_plain,
        queries,
        positions,
    )
    attended = (numerator / jnp.transpose(denominator)[:, :, None]).astype(jnp.bfloat16)
    attended = attended.reshape(row_count, head_count * VDIM)
    term = jnp.dot(pool_out, w_out_pool, preferred_element_type=jnp.float32)
    return lax.psum_scatter(
        (term + jnp.dot(attended, w_out_attn, preferred_element_type=jnp.float32)).astype(
            jnp.bfloat16
        ),
        "tp",
        scatter_dimension=0,
        tiled=True,
    )


def solution(mesh):
    placed = (
        P(("sp", "tp"), None),
        P(),
        P(None, "tp"),
        P("tp"),
        P(None, "tp"),
        P(None, "tp"),
        P(),
        P(),
        P(),
        P(None, "tp"),
        P(None, "tp"),
        P(None, "tp"),
        P(),
        P(),
        P("tp", None),
        P("tp", None),
    )
    return jax.shard_map(
        local, mesh=mesh, in_specs=placed, out_specs=P(("sp", "tp"), None), check_vma=False
    )
```

profile of v0, /device:TPU:8, one launch (start us, length us, event | category | flops | bytes accessed | tf_op | source)
XLA Modules:
  0.0 467.7 jit_solution(14622654200361501160)
XLA Ops:
  6.5 0.7 all-gather.4.cloned.1.call-update
  7.3 35.0 %all-gather.4.cloned.1.call-done = bf16[768,2048]{1,0:T(8,128)(2,1)} async-done(((bf16[96,2048]{1,0:T(8,128)(2,1)}), bf16[768,2048]{1,0:T(8,128)(2,1)}) %all-gather.4.cloned.1.call-update) | async-done | bytes 3145744 | tf_op jit(solution)/shard_map/all_gather | solution.py:170
  42.3 2.7 fusion.23
  45.1 1.5 fusion.25
  46.7 1.1 multiply_reduce_fusion.1
  47.8 1.1 multiply_reduce_fusion
  49.6 3.3 all-to-all-start
  53.0 0.8 dynamic_slice.16
  53.8 4.6 all-to-all-done
  58.5 0.7 multiply_convert_fusion
  59.3 0.8 dynamic_slice.15
  60.1 3.0 convolution_convert_fusion.6
  63.1 14.2 %all_gather.13 = bf16[768,512]{0,1:T(8,128)(2,1)S(1)} all-gather(bf16[768,64]{0,1:T(8,128)(2,1)S(1)} %multiply_convert_fusion.1), channel_id=1, replica_groups=mesh['sp'=32,'tp'=8] {'tp'}, dimensions={1}, use_global_device_ids=true | all-gather | bytes 884736 | tf_op jit(solution)/shard_map/all_gather | solution.py:196
  78.0 0.8 pad_maximum_fusion.1
  79.4 2.9 convolution_convert_fusion.1
  82.3 3.6 collective-permute-start
  85.9 1.9 collective-permute-done
  87.9 4.2 fusion.49
  92.1 1.7 convolution_convert_fusion
  94.1 119.7 %all-gather.6.cloned.1.call-done = bf16[24576,288]{0,1:T(8,128)(2,1)} async-done(((bf16[768,288]{0,1:T(8,128)(2,1)}), bf16[24576,288]{0,1:T(8,128)(2,1)}) %all-gather.6.cloned.1.call-update) | async-done | bytes 14155792 | tf_op jit(solution)/shard_map/all_gather | solution.py:46
  213.8 1.5 split.14
  215.3 10.4 %fusion.79 = (bf16[24576,128]{0,1:T(8,128)(2,1)}, bf16[24576,128]{0,1:T(8,128)(2,1)}) fusion(bf16[24576,288]{0,1:T(8,128)(2,1)} %all-gather.6.cloned.1.call-done), kind=kLoop, calls=%fused_computation.156 | loop fusion | bytes 25165824 | tf_op jit(solution)/shard_map/split | solution.py:47
  225.7 54.0 %while.15 = (s32[]{:T(128)}, f32[768,2,64]{0,2,1:T(8,128)S(1)}, f32[2,768]{1,0:T(2,128)S(1)}, s32[768]{0:T(1024)S(1)}, bf16[24576,128]{0,1:T(8,128)(2,1)}, /*ind...) while((s32[]{:T(128)}, f32[768,2,64]{0,2,1:T(8,128)S(1)}, ...), condition=%wide.region_10.11_spmd, body=%wide.region_5.10_spmd.sunk | while | flops 388119616 | bytes 15941421 | solution.py:149
  225.7 0.7 slice.283
  227.1 4.7 %conditional.2 = ((f32[768,2,64]{0,2,1:T(8,128)S(1)}, f32[2,768]{1,0:T(2,128)S(1)})) conditional(s32[]{:T(128)} %convert_element_type.159, (f32[768,2,64]{0,2,1:T(8,128)S(1)}, f32[2,768]{1,0:T(2,128)S(1)}) %tuple.56, (s32[]{:T(128)}, bf16[24576,128]{0,1:T(8,128)(2,1)}, s32[768]{0:T(1024)S(1)}, bf16[24576,128]{0,1:T(8,128)(2,1)}, ...), branch_computations={%region_6.6_spmd, %region_7.9_spmd} | conditional | flops 388119616 | bytes 15941190 | solution.py:147
  227.2 1.1 constant_dynamic-slice_fusion.1
  229.2 1.4 fusion
  230.5 1.2 fusion.8
  231.8 0.7 slice.283
  233.2 4.7 %conditional.2 = ((f32[768,2,64]{0,2,1:T(8,128)S(1)}, f32[2,768]{1,0:T(2,128)S(1)})) conditional(s32[]{:T(128)} %convert_element_type.159, (f32[768,2,64]{0,2,1:T(8,128)S(1)}, f32[2,768]{1,0:T(2,128)S(1)}) %tuple.56, (s32[]{:T(128)}, bf16[24576,128]{0,1:T(8,128)(2,1)}, s32[768]{0:T(1024)S(1)}, bf16[24576,128]{0,1:T(8,128)(2,1)}, ...), branch_computations={%region_6.6_spmd, %region_7.9_spmd} | conditional | flops 388119616 | bytes 15941190 | solution.py:147
  233.3 1.1 constant_dynamic-slice_fusion.1
  235.3 1.4 fusion
  236.6 1.2 fusion.8
  237.9 0.7 slice.283
  239.3 0.7 slice.283
  240.7 0.7 slice.283
  242.1 0.7 slice.283
  243.5 0.7 slice.283
  244.9 0.7 slice.283
  246.3 0.7 slice.283
  247.7 0.7 slice.283
  249.1 0.7 slice.283
  251.9 0.7 slice.283
  253.2 0.7 slice.283
  254.6 0.7 slice.283
  256.0 0.7 slice.283
  279.8 5.4 %add_convert_fusion.1 = bf16[768,2048]{1,0:T(8,128)(2,1)} fusion(f32[768,2048]{1,0:T(8,128)} %fusion.49, bf16[768,128]{0,1:T(8,128)(2,1)S(1)} %bitcast.48, bf16[128,2048]{1,0:T(8,128)(2,1)S(1)} %copy-done.3), kind=kOutput, calls=%fused_computation.39 | convolution fusion | flops 405798912 | bytes 10158080 | tf_op jit(solution)/shard_map/dot_general | solution.py:220
  285.2 175.9 %reduce-scatter.2.cloned.1.call-done = bf16[96,2048]{1,0:T(8,128)(2,1)} async-done(((bf16[768,2048]{1,0:T(8,128)(2,1)}), bf16[96,2048]{1,0:T(8,128)(2,1)}) %reduce-scatter.2.cloned.1.call-update) | async-done | bytes 393232 | tf_op jit(solution)/shard_map/reduce_scatter | solution.py:219
  (140 shorter events, 16.0 us)
Async XLA Ops:
  6.5 81.3 %copy-start = (bf16[128,2048]{1,0:T(8,128)(2,1)S(1)}, bf16[128,2048]{1,0:T(8,128)(2,1)}, u32[]{:S(2)}) copy-start(bf16[128,2048]{1,0:T(8,128)(2,1)} %param.34) | copy-start | bytes 1572868
  6.5 35.8 %all-gather.4.cloned.1.call-start = ((), (), s32[]{:S(2)}) async-start(), calls=%async_computation.2 | async-start | bytes 3538944 | tf_op jit(solution)/shard_map/all_gather | solution.py:170
  42.3 2.8 copy-start.2
  42.3 4.4 copy-start.6
  45.1 2.7 copy-start.4
  46.7 2.2 copy-start.1
  46.7 13.4 %copy-start.7 = (bf16[2048,32]{0,1:T(8,128)(2,1)S(1)}, bf16[2048,32]{0,1:T(8,128)(2,1)}, u32[]{:S(2)}) copy-start(bf16[2048,32]{0,1:T(8,128)(2,1)} %param.26) | copy-start | bytes 393220
  48.9 28.4 %copy-start.8 = (bf16[512,128]{1,0:T(8,128)(2,1)S(1)}, bf16[512,128]{1,0:T(8,128)(2,1)}, u32[]{:S(2)}) copy-start(bf16[512,128]{1,0:T(8,128)(2,1)} %param.31) | copy-start | bytes 393220
  48.9 28.7 %copy-start.9 = (bf16[512,128]{1,0:T(8,128)(2,1)S(1)}, bf16[512,128]{1,0:T(8,128)(2,1)}, u32[]{:S(2)}) copy-start(bf16[512,128]{1,0:T(8,128)(2,1)} %param.30) | copy-start | bytes 393220
  49.6 8.8 %all-to-all-start = ((f32[8,1,1536]{2,1,0:T(1,128)}), f32[8,1,1536]{2,1,0:T(1,128)S(1)}, u32[]{:S(2)}, u32[]{:S(2)}) async-start(f32[8,1,1536]{2,1,0:T(1,128)} %broadcast_in_dim.188), calls=%async_computation | async-start | bytes 98304 | tf_op jit(solution)/shard_map/all_to_all | solution.py:27
  53.0 39.1 %all-gather.8.cloned.1.call-start = ((), (), s32[]{:S(2)}) async-start(), calls=%async_computation.4 | async-start | bytes 1327104 | tf_op jit(solution)/shard_map/all_gather | solution.py:195
  59.3 154.5 %all-gather.6.cloned.1.call-start = ((), (), s32[]{:S(2)}) async-start(), calls=%async_computation.3 | async-start | bytes 14598144 | tf_op jit(solution)/shard_map/all_gather | solution.py:46
  60.1 19.3 %copy-start.12 = (bf16[2048,128]{1,0:T(8,128)(2,1)S(1)}, bf16[2048,128]{1,0:T(8,128)(2,1)}, u32[]{:S(2)}) copy-start(bf16[2048,128]{1,0:T(8,128)(2,1)} %param.22) | copy-start | bytes 1572868
  77.4 10.5 %copy-start.13 = (f32[128]{0:T(128)S(1)}, f32[128]{0:T(128)}, u32[]{:S(2)}) copy-start(f32[128]{0:T(128)} %param.23) | copy-start | bytes 1540
  78.9 382.3 %reduce-scatter.2.cloned.1.call-start = ((), (), s32[]{:S(2)}) async-start(), calls=%async_computation.5 | async-start | bytes 3538944 | tf_op jit(solution)/shard_map/reduce_scatter | solution.py:219
  82.3 5.5 %collective-permute-start = (bf16[15,128]{1,0:T(8,128)(2,1)S(1)}, bf16[15,128]{1,0:T(8,128)(2,1)S(1)}, u32[]{:S(2)}, u32[]{:S(2)}) collective-permute-start(bf16[15,128]{1,0:T(8,128)(2,1)S(1)} %slice.110), channel_id=1, source_target_pairs={{0,8},{8,16},{16,24},{24,32},{32,40},{40,48},{48,56},{56,64},{64,7... | collective-permute-start | bytes 11528 | tf_op jit(solution)/shard_map/ppermute | solution.py:22
  87.9 4.2 copy-start.5
  87.9 6.0 %copy-start.11 = (f32[96]{0:T(128)S(1)}, f32[96]{0:T(128)}, u32[]{:S(2)}) copy-start(f32[96]{0:T(128)} %param.32) | copy-start | bytes 1156
  215.3 10.4 %copy-start.10 = (f32[96]{0:T(128)S(1)}, f32[96]{0:T(128)}, u32[]{:S(2)}) copy-start(f32[96]{0:T(128)} %param.33) | copy-start | bytes 1156
  225.7 54.0 %copy-start.3 = (bf16[128,2048]{1,0:T(8,128)(2,1)S(1)}, bf16[128,2048]{1,0:T(8,128)(2,1)}, u32[]{:S(2)}) copy-start(bf16[128,2048]{1,0:T(8,128)(2,1)} %param.35) | copy-start | bytes 1572868
Sparse Core Ops, SparseCore 0:
  9.2 33.0 all-gather.3
  59.4 26.1 all-gather.7
  88.2 125.5 all-gather.5
  285.3 175.7 reduce-scatter.1
where the time goes:
time: 469 us; the launch traced here: 468 us
  waiting for transfers between devices  338 us (72%)
  local copies, waits for them, and re-layouts  37.6 us (8%)
  matrix products  25.2 us (5%)
  loops' own time  23.6 us (5%)
  blocking collectives  14.2 us (3%)
  between operations  13.5 us (3%)
  other arithmetic  8.52 us (2%)
  starting transfers between devices  7.03 us (1%)
    reduce_scatter x1, waiting for transfers between devices, local(): lax.psum_scatter((term + jnp.dot(attended, w_out_attn, preferred_element_...  176 us
    all_gather x1, waiting for transfers between devices, side_by_side(): filled = lax.all_gather(both, axis, axis=dim, tiled=True)  120 us
    all_gather x1, waiting for transfers between devices, local(): own_input = lax.all_gather(activations, 'tp', axis=0, tiled=True)  35 us
    another operation x1, loops' own time, sweep(): return lax.fori_loop(0, piece_rows // block_size, advance, state_pair)  23.1 us
    slice x32, local copies, waits for them, and re-layouts, advance(): return lax.cond(offset <= query_pos[-1], accumulate, unchanged, current)  21.2 us
    all_gather x1, blocking collectives, local(): lax.all_gather(kv_scaled.astype(jnp.bfloat16), 'tp', axis=1, tiled=True)  14.2 us
    split x2, local copies, waits for them, and re-layouts, side_by_side(): jnp.split(filled, [sum(widths[:k]) for k in range(1, len(widths))], axis=...  11.9 us
  transfers between devices with their start and end apart: 6, of which 5 were waited for; matrix products, arithmetic and copies ran while one was open for 3% of the time, Pallas kernels for 0%

commit v1 on v0

--- a/solution.py
+++ b/solution.py
@@ -1,3 +1,4 @@
+import functools
 import math
 import jax
 import jax.numpy as jnp
@@ -14,6 +15,18 @@
 rope_theta = 10000.0
 rim_depth = 15
 block_rows = 512
+
+
+def store_the_trails(array_in, at_axis):
+    return jnp.concatenate(
+        lax.all_to_all(
+            jnp.stack(lax.axis_size("tp") * [array_in]), axis_name="tp", split_axis=0, concat_axis=0
+        ),
+        at_axis,
+    )
+
+
+_handle_screen = functools.partial(store_the_trails, at_axis=0)
 
 
 def from_behind(block, axis, distance):
@@ -167,7 +180,7 @@
     w_out_pool,
     w_out_attn,
 ):
-    own_input = lax.all_gather(activations, "tp", axis=0, tiled=True)
+    own_input = _handle_screen(activations)
     row_count = own_input.shape[0]
     positions = lax.axis_index("sp") * row_count + jnp.arange(row_count, dtype=jnp.int32)
     normed = row_norm(own_input, in_gain).astype(jnp.bfloat16)

time: 469 us -> 473 us (level)
  blocking collectives: 14.2 us -> 55.9 us
  waiting for transfers between devices: 338 us -> 304 us
    all_to_all x0 -> x1, blocking collectives: none -> 42.5 us  [store_the_trails(): lax.all_to_all(jnp.stack(lax.axis_size('tp') * [array_in]), axis_name='tp...]
    all_gather x1 -> x0, waiting for transfers between devices: 35 us -> none  [local(): own_input = lax.all_gather(activations, 'tp', axis=0, tiled=True)]
  transfers between devices with their start and end apart: 6 -> 5, of which waited for: 5 -> 4; matrix products, arithmetic and copies ran while one was open for 3% -> 3% of each run, Pallas kernels for 0% -> 0%
where the time goes in v1:
time: 473 us; the launch traced here: 472 us
  waiting for transfers between devices  304 us (64%)
  blocking collectives  55.9 us (12%)
  local copies, waits for them, and re-layouts  38.3 us (8%)
  matrix products  25.2 us (5%)
  loops' own time  19.8 us (4%)
  between operations  13.5 us (3%)
  other arithmetic  7.69 us (2%)
  starting transfers between devices  7.14 us (2%)
    reduce_scatter x1, waiting for transfers between devices, local(): lax.psum_scatter((term + jnp.dot(attended, w_out_attn, preferred_element_...  176 us
    all_gather x1, waiting for transfers between devices, side_by_side(): filled = lax.all_gather(both, axis, axis=dim, tiled=True)  122 us
    all_to_all x1, blocking collectives, store_the_trails(): lax.all_to_all(jnp.stack(lax.axis_size('tp') * [array_in]), axis_name='tp...  42.5 us
    another operation x1, loops' own time, sweep(): return lax.fori_loop(0, piece_rows // block_size, advance, state_pair)  19.3 us
    slice x32, local copies, waits for them, and re-layouts, advance(): return lax.cond(offset <= query_pos[-1], accumulate, unchanged, current)  18.7 us
    all_gather x1, blocking collectives, local(): lax.all_gather(kv_scaled.astype(jnp.bfloat16), 'tp', axis=1, tiled=True)  13.4 us
    split x2, local copies, waits for them, and re-layouts, side_by_side(): jnp.split(filled, [sum(widths[:k]) for k in range(1, len(widths))], axis=...  11.9 us
  transfers between devices with their start and end apart: 5, of which 4 were waited for; matrix products, arithmetic and copies ran while one was open for 3% of the time, Pallas kernels for 0%

profile of v1, /device:TPU:8, one launch (start us, length us, event | category | flops | bytes accessed | tf_op | source)
XLA Modules:
  0.0 472.0 jit_solution(7645813855571118134)
XLA Ops:
  6.5 1.4 stack.2
  8.0 42.5 %all_to_all.11 = bf16[8,96,2048]{2,1,0:T(8,128)(2,1)S(1)} all-to-all(bf16[8,96,2048]{2,1,0:T(8,128)(2,1)S(1)} %stack.2), channel_id=1, replica_groups=mesh['sp'=32,'tp'=8] {'tp'}, dimensions={0} | all-to-all | bytes 6291456 | tf_op jit(solution)/shard_map/all_to_all | solution.py:22
  50.5 1.6 copy-done.2
  52.2 0.7 multiply_reduce_fusion
  53.0 2.7 fusion.24
  55.7 1.1 multiply_reduce_fusion.2
  56.8 1.1 multiply_reduce_fusion.1
  58.0 0.6 broadcast_in_dim.188
  58.7 3.3 all-to-all-start.1
  62.1 0.8 dynamic_slice.16
  62.8 4.6 all-to-all-done.1
  67.5 0.7 multiply_convert_fusion
  68.3 0.8 dynamic_slice.15
  69.1 3.0 convolution_convert_fusion.6
  72.2 13.4 %all_gather.9 = bf16[768,512]{0,1:T(8,128)(2,1)S(1)} all-gather(bf16[768,64]{0,1:T(8,128)(2,1)S(1)} %multiply_convert_fusion.1), channel_id=1, replica_groups=mesh['sp'=32,'tp'=8] {'tp'}, dimensions={1}, use_global_device_ids=true | all-gather | bytes 884736 | tf_op jit(solution)/shard_map/all_gather | solution.py:209
  86.2 0.8 pad_maximum_fusion.1
  87.6 2.9 convolution_convert_fusion.1
  90.5 3.7 collective-permute-start
  94.2 1.8 collective-permute-done
  96.1 4.2 fusion.48
  100.3 1.7 convolution_convert_fusion
  102.3 122.1 %all-gather.3.cloned.1.call-done = bf16[24576,288]{0,1:T(8,128)(2,1)} async-done(((bf16[768,288]{0,1:T(8,128)(2,1)}), bf16[24576,288]{0,1:T(8,128)(2,1)}) %all-gather.3.cloned.1.call-update) | async-done | bytes 14155792 | tf_op jit(solution)/shard_map/all_gather | solution.py:59
  224.3 1.5 split.14
  225.9 10.4 %fusion.78 = (bf16[24576,128]{0,1:T(8,128)(2,1)}, bf16[24576,128]{0,1:T(8,128)(2,1)}) fusion(bf16[24576,288]{0,1:T(8,128)(2,1)} %all-gather.3.cloned.1.call-done), kind=kLoop, calls=%fused_computation.155 | loop fusion | bytes 25165824 | tf_op jit(solution)/shard_map/split | solution.py:60
  236.3 47.8 %while.15 = (s32[]{:T(128)}, f32[768,2,64]{0,2,1:T(8,128)S(1)}, f32[2,768]{1,0:T(2,128)S(1)}, s32[768]{0:T(1024)S(1)}, bf16[24576,128]{0,1:T(8,128)(2,1)}, /*ind...) while((s32[]{:T(128)}, f32[768,2,64]{0,2,1:T(8,128)S(1)}, ...), condition=%wide.region_10.11_spmd, body=%wide.region_5.10_spmd.sunk | while | flops 388119616 | bytes 15941421 | solution.py:162
  236.4 0.6 slice.283
  237.5 4.7 %conditional.2 = ((f32[768,2,64]{0,2,1:T(8,128)S(1)}, f32[2,768]{1,0:T(2,128)S(1)})) conditional(s32[]{:T(128)} %convert_element_type.162, (f32[768,2,64]{0,2,1:T(8,128)S(1)}, f32[2,768]{1,0:T(2,128)S(1)}) %tuple.56, (s32[]{:T(128)}, bf16[24576,128]{0,1:T(8,128)(2,1)}, s32[768]{0:T(1024)S(1)}, bf16[24576,128]{0,1:T(8,128)(2,1)}, ...), branch_computations={%region_6.6_spmd, %region_7.9_spmd} | conditional | flops 388119616 | bytes 15941190 | solution.py:160
  237.6 1.1 constant_dynamic-slice_fusion.1
  239.6 1.4 fusion
  241.0 1.2 fusion.8
  242.3 0.6 slice.283
  243.4 4.7 conditional.2
  243.5 1.1 constant_dynamic-slice_fusion.1
  245.5 1.4 fusion
  246.9 1.2 fusion.8
  248.2 0.6 slice.283
  250.6 0.6 slice.283
  251.8 0.6 slice.283
  253.0 0.6 slice.283
  254.2 0.6 slice.283
  255.4 0.6 slice.283
  256.6 0.6 slice.283
  257.8 0.6 slice.283
  260.2 0.6 slice.283
  261.4 0.6 slice.283
  262.6 0.6 slice.283
  284.2 5.4 %add_convert_fusion.1 = bf16[768,2048]{1,0:T(8,128)(2,1)} fusion(f32[768,2048]{1,0:T(8,128)} %fusion.48, bf16[768,128]{0,1:T(8,128)(2,1)S(1)} %bitcast.54, bf16[128,2048]{1,0:T(8,128)(2,1)S(1)} %copy-done.3), kind=kOutput, calls=%fused_computation.37 | convolution fusion | flops 405798912 | bytes 10158080 | tf_op jit(solution)/shard_map/dot_general | solution.py:233
  289.6 175.9 %reduce-scatter.2.cloned.1.call-done = bf16[96,2048]{1,0:T(8,128)(2,1)} async-done(((bf16[768,2048]{1,0:T(8,128)(2,1)}), bf16[96,2048]{1,0:T(8,128)(2,1)}) %reduce-scatter.2.cloned.1.call-update) | async-done | bytes 393232 | tf_op jit(solution)/shard_map/reduce_scatter | solution.py:232
  (142 shorter events, 15.2 us)
Async XLA Ops:
  6.5 89.5 %copy-start = (bf16[128,2048]{1,0:T(8,128)(2,1)S(1)}, bf16[128,2048]{1,0:T(8,128)(2,1)}, u32[]{:S(2)}) copy-start(bf16[128,2048]{1,0:T(8,128)(2,1)} %param.34) | copy-start | bytes 1572868
  8.0 45.0 %copy-start.11 = (f32[2048]{0:T(1024)S(1)}, f32[2048]{0:T(1024)}, u32[]{:S(2)}) copy-start(f32[2048]{0:T(1024)} %param.21) | copy-start | bytes 24580
  50.5 1.6 copy-start.2
  52.2 3.5 copy-start.6
  53.0 3.9 copy-start.4
  55.7 2.3 copy-start.1
  55.7 13.4 %copy-start.7 = (bf16[2048,32]{0,1:T(8,128)(2,1)S(1)}, bf16[2048,32]{0,1:T(8,128)(2,1)}, u32[]{:S(2)}) copy-start(bf16[2048,32]{0,1:T(8,128)(2,1)} %param.26) | copy-start | bytes 393220
  58.0 27.6 %copy-start.8 = (bf16[512,128]{1,0:T(8,128)(2,1)S(1)}, bf16[512,128]{1,0:T(8,128)(2,1)}, u32[]{:S(2)}) copy-start(bf16[512,128]{1,0:T(8,128)(2,1)} %param.31) | copy-start | bytes 393220
  58.0 27.9 %copy-start.9 = (bf16[512,128]{1,0:T(8,128)(2,1)S(1)}, bf16[512,128]{1,0:T(8,128)(2,1)}, u32[]{:S(2)}) copy-start(bf16[512,128]{1,0:T(8,128)(2,1)} %param.30) | copy-start | bytes 393220
  58.7 8.8 %all-to-all-start.1 = ((f32[8,1,1536]{2,1,0:T(1,128)}), f32[8,1,1536]{2,1,0:T(1,128)S(1)}, u32[]{:S(2)}, u32[]{:S(2)}) async-start(f32[8,1,1536]{2,1,0:T(1,128)} %broadcast_in_dim.188), calls=%async_computation.1 | async-start | bytes 98304 | tf_op jit(solution)/shard_map/all_to_all | solution.py:40
  62.0 38.3 %all-gather.5.cloned.1.call-start = ((), (), s32[]{:S(2)}) async-start(), calls=%async_computation.4 | async-start | bytes 1327104 | tf_op jit(solution)/shard_map/all_gather | solution.py:208
  68.3 156.0 %all-gather.3.cloned.1.call-start = ((), (), s32[]{:S(2)}) async-start(), calls=%async_computation.3 | async-start | bytes 14598144 | tf_op jit(solution)/shard_map/all_gather | solution.py:59
  69.1 18.5 %copy-start.13 = (bf16[2048,128]{1,0:T(8,128)(2,1)S(1)}, bf16[2048,128]{1,0:T(8,128)(2,1)}, u32[]{:S(2)}) copy-start(bf16[2048,128]{1,0:T(8,128)(2,1)} %param.22) | copy-start | bytes 1572868
  85.6 10.5 %copy-start.14 = (f32[128]{0:T(128)S(1)}, f32[128]{0:T(128)}, u32[]{:S(2)}) copy-start(f32[128]{0:T(128)} %param.23) | copy-start | bytes 1540
  87.1 378.4 %reduce-scatter.2.cloned.1.call-start = ((), (), s32[]{:S(2)}) async-start(), calls=%async_computation.5 | async-start | bytes 3538944 | tf_op jit(solution)/shard_map/reduce_scatter | solution.py:232
  90.5 5.5 %collective-permute-start = (bf16[15,128]{1,0:T(8,128)(2,1)S(1)}, bf16[15,128]{1,0:T(8,128)(2,1)S(1)}, u32[]{:S(2)}, u32[]{:S(2)}) collective-permute-start(bf16[15,128]{1,0:T(8,128)(2,1)S(1)} %slice.110), channel_id=1, source_target_pairs={{0,8},{8,16},{16,24},{24,32},{32,40},{40,48},{48,56},{56,64},{64,7... | collective-permute-start | bytes 11528 | tf_op jit(solution)/shard_map/ppermute | solution.py:35
  96.0 4.2 copy-start.5
  96.1 6.0 %copy-start.12 = (f32[96]{0:T(128)S(1)}, f32[96]{0:T(128)}, u32[]{:S(2)}) copy-start(f32[96]{0:T(128)} %param.32) | copy-start | bytes 1156
  225.9 10.5 %copy-start.10 = (f32[96]{0:T(128)S(1)}, f32[96]{0:T(128)}, u32[]{:S(2)}) copy-start(f32[96]{0:T(128)} %param.33) | copy-start | bytes 1156
  236.3 47.8 %copy-start.3 = (bf16[128,2048]{1,0:T(8,128)(2,1)S(1)}, bf16[128,2048]{1,0:T(8,128)(2,1)}, u32[]{:S(2)}) copy-start(bf16[128,2048]{1,0:T(8,128)(2,1)} %param.35) | copy-start | bytes 1572868
Sparse Core Ops, SparseCore 0:
  68.4 26.9 all-gather.4
  98.1 126.2 all-gather.2
  289.8 175.7 reduce-scatter.1
